TPU v7x, 32 devices: a whole 2x2x4 slice. The times are simulated.
32 devices in a mesh: ra: 8 (over z, y), cb: 4 (over x, core).
Axes of the slice: x: 2, y: 2, z: 4, core: 2. Of those that a mesh axis runs over, the one named last changes fastest.
Arguments:
- tokens: bfloat16 [4, 128, 4096], P(None, None, 'ra'), may hold values from -64 to 64
- norm_gain: float32 [2, 4096], P(None, 'ra'), may hold values from 0.1 to 1.9
- gate_weight: bfloat16 [2, 4096, 11264], P(None, 'ra', 'cb'), may hold values from -0.09375 to 0.09375
- up_weight: bfloat16 [2, 4096, 11264], P(None, 'ra', 'cb'), may hold values from -0.09375 to 0.09375
- gate_taps: float32 [2, 3, 11264], P(None, None, 'cb'), may hold values from -3 to 3
- up_taps: float32 [2, 3, 11264], P(None, None, 'cb'), may hold values from -3 to 3
- gate_bias: float32 [2, 11264], P(None, 'cb'), may hold values from -3 to 3
- up_bias: float32 [2, 11264], P(None, 'cb'), may hold values from -3 to 3
- down_weight: bfloat16 [2, 11264, 4096], P(None, 'cb', 'ra'), may hold values from -0.0546875 to 0.0546875
Outputs:
- mixed: bfloat16 [4, 128, 4096], P(None, None, 'ra')
All inputs are finite; a program needn't handle non-finite values.
Results may differ from a plain program's by a relative error of at most 0.03.
Values may be sent and summed in bfloat16 or wider, within the bound.
A program may use at most 64 MiB of HBM per device.

v0:
```python
import functools

import jax
import jax.numpy as jnp
from jax import lax
from jax.experimental import pallas as pl
from jax.experimental.pallas import tpu as pltpu
from jax.sharding import PartitionSpec as P

EPS = 1e-06
RESID = 0.5
GROUPS = 2
STAGES = (("project", 0), ("add_y", 2), ("fold", 3), ("activate", 4),
          ("spread_z", 5), ("spread_y", 6), ("down", 8))
STAGES = tuple((lag, stage) for stage, lag in STAGES)
TAILS = ((0, "reduce_start"), (1, "reduce_end"), (2, "finish"), (3, "settle"))

MESH = pl.DeviceIdType.MESH
F32, BF16 = jnp.float32, jnp.bfloat16


def kernel(
    dims,
    tok_ref, gain_ref, gw_hbm, uw_hbm, gt_ref, ut_ref, gb_ref, ub_ref, dw_hbm,
    out_ref,
    gw_ref, uw_ref, dw_ref, carried, scaled, inv, tmp, acc,
    sq_own, sq_in, part, y_in, zpart, z_in, zfold, zf_in, hid, c_out, c_in, c_all,
    w_sem, sq_s, sq_r, y_s, y_r, z_s, z_r, hz_s, hz_r, hy_s, hy_r, c_s, c_r, ca_s, ca_r,
):
    n_ra, n_cb, nz, groups, rows, length, layers, width, chunks = dims
    ny = n_ra // nz
    total_chunks = layers * groups * chunks
    cb_rows = rows // n_cb
    me_ra = lax.axis_index("ra")
    me_cb = lax.axis_index("cb")
    me_z, me_y = me_ra // ny, me_ra % ny

    def weight_copies(layer):
        return [
            pltpu.make_async_copy(src.at[layer], dst.at[layer], w_sem.at[layer, k])
            for k, (src, dst) in enumerate(
                [(gw_hbm, gw_ref), (uw_hbm, uw_ref), (dw_hbm, dw_ref)]
            )
        ]

    for layer in range(layers):
        for copy in weight_copies(layer):
            copy.start()

    barrier = pltpu.get_barrier_semaphore()
    for step in range(1, n_ra):
        pl.semaphore_signal(
            barrier, inc=1, device_id={"ra": lax.rem(me_ra + step, n_ra)}, device_id_type=MESH
        )
    for step in range(1, n_cb):
        pl.semaphore_signal(
            barrier, inc=1, device_id={"cb": lax.rem(me_cb + step, n_cb)}, device_id_type=MESH
        )

    def remote(src, dst, send, recv, **where):
        return pltpu.make_async_remote_copy(
            src_ref=src, dst_ref=dst, send_sem=send, recv_sem=recv,
            device_id=where, device_id_type=MESH,
        )

    def square_copy(g, step):
        return remote(
            sq_own.at[g], sq_in.at[g, step - 1], sq_s.at[g, step - 1], sq_r.at[g, step - 1],
            ra=lax.rem(me_ra + step, n_ra),
        )

    def y_copy(g, i, step):
        to = lax.rem(me_y + step, ny)
        return remote(
            part.at[g, i, to], y_in.at[g, i, step - 1],
            y_s.at[g, i, step - 1], y_r.at[g, i, step - 1], ra=me_z * ny + to,
        )

    side, half_z = me_z % 2, me_z // 2
    my_block = 2 * side + half_z
    near = (me_z + 1 - 2 * side) * ny + me_y
    far = (me_z + 2 - 4 * half_z) * ny + me_y

    def near_copy(g, i):
        return remote(
            zpart.at[g, i, pl.ds(2 * (1 - side), 2)], z_in.at[g, i],
            z_s.at[g, i, 0], z_r.at[g, i, 0], ra=near,
        )

    def far_copy(g, i):
        return remote(
            zfold.at[g, i, 1 - half_z], zf_in.at[g, i],
            z_s.at[g, i, 1], z_r.at[g, i, 1], ra=far,
        )

    def hfar_copy(g, i, block):
        block = hid.at[g, i, me_y, block]
        return remote(block, block, hz_s.at[g, i, 0], hz_r.at[g, i, 0], ra=far)

    def hnear_copy(g, i, first):
        block = hid.at[g, i, me_y, pl.ds(2 * first, 2)]
        return remote(block, block, hz_s.at[g, i, 1], hz_r.at[g, i, 1], ra=near)

    def hy_copy(g, i, step, y):
        to = lax.rem(me_y + step, ny)
        block = hid.at[g, i, y]
        return remote(
            block, block, hy_s.at[g, i, step - 1], hy_r.at[g, i, step - 1], ra=me_z * ny + to
        )

    def c_copy(g, step):
        to = lax.rem(me_cb + step, n_cb)
        return remote(
            c_out.at[g, to], c_in.at[g, step - 1], c_s.at[g, step - 1], c_r.at[g, step - 1], cb=to
        )

    def ca_copy(g, step, block):
        to = lax.rem(me_cb + step, n_cb)
        block = c_all.at[g, block]
        return remote(block, block, ca_s.at[g, step - 1], ca_r.at[g, step - 1], cb=to)

    row_in_seq = lax.broadcasted_iota(jnp.int32, (length, width), 0)

    def prepare(layer, g):
        values = carried[g]
        squares = jnp.sum(values * values, axis=1, keepdims=True)
        sq_own[g] = jnp.transpose(jnp.broadcast_to(squares, (rows, 128)))[:8]
        for step in range(1, n_ra):
            square_copy(g, step).start()
        scaled[g] = (values * gain_ref[layer]).astype(BF16)
        acc[g] = jnp.zeros(acc.shape[1:], F32)

    def scale(g):
        total = sq_own[g]
        for step in range(1, n_ra):
            square_copy(g, step).wait()
            total = total + sq_in[g, step - 1]
        total = jnp.transpose(jnp.concatenate([total] * 16, axis=0))
        inv[g] = lax.rsqrt(total / (n_ra * gain_ref.shape[2]) + EPS)

    def project(layer, g, i):
        cols = pl.ds(pl.multiple_of(i * width, width), width)
        for half, (w_ref, taps) in enumerate([(gw_ref, gt_ref), (uw_ref, ut_ref)]):
            lanes = slice(half * width, (half + 1) * width)
            tmp[...] = jnp.dot(scaled[g], w_ref[layer, :, cols], preferred_element_type=F32)
            tap = [taps[layer, pl.ds(k, 1), cols] for k in range(3)]
            for s in range(rows // length):
                span = slice(s * length, (s + 1) * length)
                pre = tmp[span, :] * inv[g, span, :1]
                last = jnp.where(row_in_seq >= 1, pltpu.roll(pre, 1, 0), 0.0)
                older = jnp.where(row_in_seq >= 2, pltpu.roll(pre, 2, 0), 0.0)
                tmp[span, :] = tap[0] * older + tap[1] * last + tap[2] * pre
            part[g, i, :, :, :, lanes] = tmp[...].astype(BF16).reshape(
                ny, nz, rows // n_ra, width
            )
        for step in range(1, ny):
            y_copy(g, i, step).start()

    def add_y(layer, g, i):
        for step in range(1, ny):
            y_copy(g, i, step).wait_recv()
        value = part[g, i, me_y].astype(F32)
        for step in range(1, ny):
            value = value + y_in[g, i, step - 1].astype(F32)
        zpart[g, i] = value.astype(BF16)
        near_copy(g, i).start()

    def fold(layer, g, i):
        near_copy(g, i).wait_recv()
        value = zpart[g, i, pl.ds(2 * side, 2)].astype(F32) + z_in[g, i].astype(F32)
        zfold[g, i] = value.astype(BF16)
        far_copy(g, i).start()

    def activate(layer, g, i):
        cols = pl.ds(pl.multiple_of(i * width, width), width)
        far_copy(g, i).wait_recv()
        value = zfold[g, i, half_z].astype(F32) + zf_in[g, i].astype(F32)
        gate = value[:, :width] + gb_ref[layer, :, cols]
        up = value[:, width:] + ub_ref[layer, :, cols]
        hid[g, i, me_y, my_block] = (gate / (1.0 + jnp.exp(-gate)) * up).astype(BF16)
        hfar_copy(g, i, my_block).start()

    def spread_z(layer, g, i):
        hfar_copy(g, i, 2 * side + 1 - half_z).wait_recv()
        hnear_copy(g, i, side).start()

    def spread_y(layer, g, i):
        hnear_copy(g, i, 1 - side).wait_recv()
        for step in range(1, ny):
            hy_copy(g, i, step, me_y).start()

    def down(layer, g, i):
        depth = pl.ds(pl.multiple_of(i * width, width), width)
        for step in range(1, ny):
            hy_copy(g, i, step, lax.rem(me_y - step + ny, ny)).wait_recv()
        acc[g] += jnp.dot(
            hid[g, i].reshape(rows, width), dw_ref[layer, depth, :], preferred_element_type=F32
        )

    def reduce_start(layer, g):
        c_out[g] = acc[g].astype(BF16).reshape(c_out.shape[1:])
        for step in range(1, n_cb):
            c_copy(g, step).start()

    def reduce_end(layer, g):
        value = acc[g, pl.ds(pl.multiple_of(me_cb * cb_rows, cb_rows), cb_rows), :]
        for step in range(1, n_cb):
            c_copy(g, step).wait()
            value = value + c_in[g, step - 1].astype(F32)
        c_all[g, me_cb] = value.astype(BF16)
        for step in range(1, n_cb):
            ca_copy(g, step, me_cb).start()

    def finish(layer, g):
        for step in range(1, n_cb):
            ca_copy(g, step, lax.rem(me_cb - step + n_cb, n_cb)).wait_recv()
            ca_copy(g, step, me_cb).wait_send()
        branch = c_all[g].reshape(rows, c_all.shape[3]).astype(F32)
        carried[g] = RESID * carried[g] + branch

        @pl.when(layer < layers - 1)
        def _():
            prepare(layer + 1, g)

    def settle(layer, g):
        def one(i, _):
            for step in range(1, ny):
                y_copy(g, i, step).wait_send()
                hy_copy(g, i, step, me_y).wait_send()
            near_copy(g, i).wait_send()
            far_copy(g, i).wait_send()
            hfar_copy(g, i, my_block).wait_send()
            hnear_copy(g, i, side).wait_send()
            return 0

        lax.fori_loop(0, chunks, one, 0)

        @pl.when(layer < layers - 1)
        def _():
            scale(g)

    carried[...] = tok_ref[...].astype(F32)
    pl.semaphore_wait(barrier, n_ra + n_cb - 2)
    for g in range(groups):
        prepare(0, g)
    for layer in range(layers):
        for copy in weight_copies(layer):
            copy.wait()
    for g in range(groups):
        scale(g)

    def body(t, _):
        for lag, stage in STAGES:
            at = t - lag
            run = at // chunks

            @pl.when((at >= 0) & (at < total_chunks))
            def _():
                stage_of[stage](run // groups, run % groups, at % chunks)

        for lag, stage in TAILS:
            at = t - STAGES[-1][0] - lag
            run = at // chunks

            @pl.when((at >= 0) & (at < total_chunks) & (at % chunks == chunks - 1))
            def _():
                stage_of[stage](run // groups, run % groups)

        return 0

    stage_of = {
        "project": project, "add_y": add_y, "activate": activate, "spread_z": spread_z,
        "spread_y": spread_y, "fold": fold,
        "down": down, "reduce_start": reduce_start, "reduce_end": reduce_end,
        "finish": finish, "settle": settle,
    }
    lax.fori_loop(0, total_chunks + STAGES[-1][0] + TAILS[-1][0], body, 0)
    out_ref[...] = carried[...].astype(out_ref.dtype)


def per_device(n_ra, n_cb, tokens, gain, gw, uw, gt, ut, gb, ub, dw):
    seqs, length, d = tokens.shape
    layers, _, ff = gw.shape
    nz = seqs
    ny = n_ra // nz
    groups = GROUPS
    rows = seqs * length // groups
    pr = rows // n_ra
    width = 256 if ff % 256 == 0 and ff // 256 >= 8 else 128
    chunks = ff // width
    dims = (n_ra, n_cb, nz, groups, rows, length, layers, width, chunks)
    vmem = pl.BlockSpec(memory_space=pltpu.VMEM)
    hbm = pl.BlockSpec(memory_space=pl.ANY)
    dma = pltpu.SemaphoreType.DMA
    ys, zs = max(ny - 1, 1), 2
    scratch = [
        pltpu.VMEM((layers, d, ff), BF16),
        pltpu.VMEM((layers, d, ff), BF16),
        pltpu.VMEM((layers, ff, d), BF16),
        pltpu.VMEM((groups, rows, d), F32),
        pltpu.VMEM((groups, rows, d), BF16),
        pltpu.VMEM((groups, rows, 128), F32),
        pltpu.VMEM((rows, width), F32),
        pltpu.VMEM((groups, rows, d), F32),
        pltpu.VMEM((groups, 8, rows), F32),
        pltpu.VMEM((groups, n_ra - 1, 8, rows), F32),
        pltpu.VMEM((groups, chunks, ny, nz, pr, 2 * width), BF16),
        pltpu.VMEM((groups, chunks, ys, nz, pr, 2 * width), BF16),
        pltpu.VMEM((groups, chunks, nz, pr, 2 * width), BF16),
        pltpu.VMEM((groups, chunks, 2, pr, 2 * width), BF16),
        pltpu.VMEM((groups, chunks, 2, pr, 2 * width), BF16),
        pltpu.VMEM((groups, chunks, pr, 2 * width), BF16),
        pltpu.VMEM((groups, chunks, ny, nz, pr, width), BF16),
        pltpu.VMEM((groups, n_cb, rows // n_cb, d), BF16),
        pltpu.VMEM((groups, n_cb - 1, rows // n_cb, d), BF16),
        pltpu.VMEM((groups, n_cb, rows // n_cb, d), BF16),
        dma((layers, 3)),
        dma((groups, n_ra - 1)), dma((groups, n_ra - 1)),
        dma((groups, chunks, ys)), dma((groups, chunks, ys)),
        dma((groups, chunks, zs)), dma((groups, chunks, zs)),
        dma((groups, chunks, zs)), dma((groups, chunks, zs)),
        dma((groups, chunks, ys)), dma((groups, chunks, ys)),
        dma((groups, n_cb - 1)), dma((groups, n_cb - 1)),
        dma((groups, n_cb - 1)), dma((groups, n_cb - 1)),
    ]
    out = pl.pallas_call(
        functools.partial(kernel, dims),
        out_shape=jax.ShapeDtypeStruct((groups, rows, d), tokens.dtype),
        in_specs=[vmem, vmem, hbm, hbm, vmem, vmem, vmem, vmem, hbm],
        out_specs=vmem,
        scratch_shapes=scratch,
        compiler_params=pltpu.CompilerParams(
            collective_id=0, has_side_effects=True, vmem_limit_bytes=60 * 1024 * 1024
        ),
        name="blocks",
    )(
        tokens.reshape(groups, rows, d), gain[:, None, :], gw, uw, gt, ut,
        gb[:, None, :], ub[:, None, :], dw,
    )
    return out.reshape(tokens.shape)


def solution(mesh):
    in_specs = (
        P(None, None, "ra"),
        P(None, "ra"),
        P(None, "ra", "cb"),
        P(None, "ra", "cb"),
        P(None, None, "cb"),
        P(None, None, "cb"),
        P(None, "cb"),
        P(None, "cb"),
        P(None, "cb", "ra"),
    )
    return jax.shard_map(
        functools.partial(per_device, mesh.shape["ra"], mesh.shape["cb"]),
        mesh=mesh, in_specs=in_specs, out_specs=P(None, None, "ra"), check_vma=False,
    )
```

profile of v0, /device:TPU:0, one launch (start us, length us, event | category | flops | bytes accessed | tf_op | source)
XLA Modules:
  0.0 229.7 jit_solution(826911339458033719)
XLA Ops:
  0.0 1.3 broadcast_in_dim.9.gain_ref
  1.3 1.4 broadcast_in_dim.10.gb_ref
  2.6 1.3 broadcast_in_dim.11.ub_ref
  4.0 1.5 copy.10.gt_ref
  5.5 1.5 copy.11.ut_ref
  7.1 220.8 %blocks.1 = bf16[2,256,512]{2,1,0:T(8,128)(2,1)} custom-call(bf16[2,256,512]{2,1,0:T(8,128)(2,1)} %bitcast.3, f32[2,1,512]{2,1,0:T(1,128)} %broadcast_in_dim.9.gain_ref, bf16[2,512,2816]{2,1,0:T(8,128)(2,1)} %gw_hbm.1, bf16[2,512,2816]{2,1,0:T(8,128)(2,1)} %uw_hbm.1, f32[2,3,2816]{2,1,0:T(4,128)} %copy.10.gt_ref, f32[2,3,2816]{2,1,0:T(4,128)} %copy.11.ut_ref, ...), custom_call_target="tpu_custom_call" | custom-call | tf_op jit(solution)/shard_map/blocks/pallas_call | solution.py:326
  227.8 1.9 copy.13
where the time goes:
time: 231 us; the launch traced here: 230 us
  Pallas kernels  221 us (96%)
  local copies, waits for them, and re-layouts  8.92 us (4%)
    pallas_call x1, Pallas kernels, per_device(): pl.pallas_call(functools.partial(kernel, dims), out_shape=jax.ShapeDtypeS...  221 us
    unnamed x3, local copies, waits for them, and re-layouts  4.95 us

commit v1 on v0

v1 whole, which is shorter than its diff:
```python
import functools

import jax
import jax.numpy as jnp
from jax import lax
from jax.experimental import pallas as pl
from jax.experimental.pallas import tpu as pltpu
from jax.sharding import PartitionSpec as P

EPS = 1e-06
RESID = 0.5
LANES = 128
CORES = 2
LAG_Y, LAG_Z, LAG_HY, LAG_HZ = 2, 2, 2, 2
TAIL_SUM, TAIL_END = 1, 4

MESH = pl.DeviceIdType.MESH
F32, BF16 = jnp.float32, jnp.bfloat16


def kernel(
    dims,
    tok_ref, gain_ref, gw_hbm, uw_hbm, gt_ref, ut_ref, gb_ref, ub_ref, dw_hbm,
    out_ref,
    gw_ref, uw_ref, dw_ref, carried, scaled, inv, acc,
    sq_own, sq_in, part, y_in, z_in, hid, c_out, c_in, c_sum,
    w_sem, sq_s, sq_r, y_s, y_r, z_s, z_r, hy_s, hy_r, hz_s, hz_r, c_s, c_r, ca_s, ca_r,
):
    n_ra, n_cb, nz, groups, rows, length, layers, width, chunks = dims
    ny = n_ra // nz
    blocks = width // LANES
    per_layer = groups * chunks
    half_rows = rows // CORES
    me_ra = lax.axis_index("ra")
    me_cb = lax.axis_index("cb")
    me_z, me_y = me_ra // ny, me_ra % ny
    core = me_cb % CORES
    seq, block = me_y // blocks, me_y % blocks

    def weight_copies(layer, i):
        cols = pl.ds(pl.multiple_of(i * width, width), width)
        return [
            pltpu.make_async_copy(
                gw_hbm.at[layer, :, cols], gw_ref.at[layer, :, cols], w_sem.at[layer, i, 0]
            ),
            pltpu.make_async_copy(
                uw_hbm.at[layer, :, cols], uw_ref.at[layer, :, cols], w_sem.at[layer, i, 1]
            ),
            pltpu.make_async_copy(
                dw_hbm.at[layer, cols], dw_ref.at[layer, cols], w_sem.at[layer, i, 2]
            ),
        ]

    for layer in range(layers):
        def fetch(i, _, layer=layer):
            for copy in weight_copies(layer, i):
                copy.start()
            return 0

        lax.fori_loop(0, chunks, fetch, 0)

    barrier = pltpu.get_barrier_semaphore()
    for step in range(1, n_ra):
        pl.semaphore_signal(
            barrier, inc=1, device_id={"ra": lax.rem(me_ra + step, n_ra)}, device_id_type=MESH
        )
    for step in range(1, n_cb):
        pl.semaphore_signal(
            barrier, inc=1, device_id={"cb": lax.rem(me_cb + step, n_cb)}, device_id_type=MESH
        )

    def remote(src, dst, send, recv, **where):
        return pltpu.make_async_remote_copy(
            src_ref=src, dst_ref=dst, send_sem=send, recv_sem=recv,
            device_id=where, device_id_type=MESH,
        )

    def square_copy(layer, g, step):
        return remote(
            sq_own.at[layer, g], sq_in.at[layer, g, step - 1],
            sq_s.at[layer, g, step - 1], sq_r.at[layer, g, step - 1],
            ra=lax.rem(me_ra + step, n_ra),
        )

    def y_copy(at, step):
        to = lax.rem(me_y + step, ny)
        return remote(
            part.at[at, to], y_in.at[at, step - 1],
            y_s.at[at, step - 1], y_r.at[at, step - 1], ra=me_z * ny + to,
        )

    def along(end):
        return lax.rem(me_z + 2 * end - 1 + nz, nz) * ny + me_y

    def z_copy(at, end):
        return remote(part.at[at, me_y], z_in.at[at], z_s.at[at], z_r.at[at], ra=along(end))

    def hy_copy(at, step, y):
        to = lax.rem(me_y + step, ny)
        block = hid.at[at, y]
        return remote(
            block, block, hy_s.at[at, step - 1], hy_r.at[at, step - 1], ra=me_z * ny + to
        )

    def hz_copy(at, end):
        return remote(hid.at[at], hid.at[at], hz_s.at[at], hz_r.at[at], ra=along(1 - end))

    def core_copy(layer, g):
        return remote(
            c_out.at[layer, g], c_in.at[layer, g], c_s.at[layer, g], c_r.at[layer, g],
            cb=me_cb + 1 - 2 * core,
        )

    def sum_copy(layer, g, step, block):
        to = lax.rem(me_cb + step, n_cb)
        block = c_sum.at[layer, g, block]
        return remote(
            block, block, ca_s.at[layer, g, step - 1], ca_r.at[layer, g, step - 1], cb=to
        )

    row_in_seq = lax.broadcasted_iota(jnp.int32, (length, LANES), 0)

    def prepare(layer, g):
        values = carried[g]
        squares = jnp.sum(values * values, axis=1, keepdims=True)
        sq_own[layer, g] = jnp.transpose(jnp.broadcast_to(squares, (rows, LANES)))[:1]
        scaled[g] = (values * gain_ref[layer]).astype(BF16)
        acc[g] = jnp.zeros(acc.shape[1:], F32)

    def send_squares(layer, g):
        for step in range(1, n_ra):
            square_copy(layer, g, step).start()

    def scale(layer, g):
        total = sq_own[layer, g]
        for step in range(1, n_ra):
            square_copy(layer, g, step).wait()
            total = total + sq_in[layer, g, step - 1]
        total = jnp.transpose(jnp.broadcast_to(total, (LANES, rows)))
        inv[g] = lax.rsqrt(total / (n_ra * gain_ref.shape[2]) + EPS)

    def project(layer, g, i, at):
        @pl.when(g == 0)
        def _():
            for copy in weight_copies(layer, i)[:2]:
                copy.wait()

        cols = pl.ds(pl.multiple_of(i * width, width), width)
        for half, w_ref in enumerate((gw_ref, uw_ref)):
            product = jnp.dot(scaled[g], w_ref[layer, :, cols], preferred_element_type=F32)
            for unit in range(ny):
                s, b = unit // blocks, unit % blocks
                part[at, unit, :, half * LANES:(half + 1) * LANES] = product[
                    s * length:(s + 1) * length, b * LANES:(b + 1) * LANES
                ].astype(BF16)
        for step in range(1, ny):
            y_copy(at, step).start()

    def add_y(at):
        value = part[at, me_y].astype(F32)
        for step in range(1, ny):
            y_copy(at, step).wait_recv()
            value = value + y_in[at, step - 1].astype(F32)
        part[at, me_y] = value.astype(BF16)

    def add_z(at, end):
        z_copy(at, end).wait_recv()
        return part[at, me_y].astype(F32) + z_in[at].astype(F32)

    def activate(layer, g, i, at, end):
        value = add_z(at, end)
        cols = pl.ds(pl.multiple_of(i * width + block * LANES, LANES), LANES)
        factor = inv[g, pl.ds(pl.multiple_of(seq * length, length), length), :]
        conv = []
        for half, (taps, bias) in enumerate(((gt_ref, gb_ref), (ut_ref, ub_ref))):
            pre = value[:, half * LANES:(half + 1) * LANES] * factor
            pre = pre.astype(BF16).astype(F32)
            last = jnp.where(row_in_seq >= 1, pltpu.roll(pre, 1, 0), 0.0)
            older = jnp.where(row_in_seq >= 2, pltpu.roll(pre, 2, 0), 0.0)
            tap = [taps[layer, pl.ds(k, 1), cols] for k in range(3)]
            conv.append(
                bias[layer, :, cols] + tap[0] * older + tap[1] * last + tap[2] * pre
            )
        gate, up = conv
        hid[at, me_y] = (gate / (1.0 + jnp.exp(-gate)) * up).astype(BF16)
        for step in range(1, ny):
            hy_copy(at, step, me_y).start()

    def gather_y(at):
        for step in range(1, ny):
            hy_copy(at, step, lax.rem(me_y - step + ny, ny)).wait_recv()

    def down(layer, g, i, at):
        @pl.when(g == 0)
        def _():
            weight_copies(layer, i)[2].wait()

        depth = pl.ds(pl.multiple_of(i * width, width), width)
        units = [hid[at, unit] for unit in range(ny)]
        hidden = jnp.concatenate(
            [jnp.concatenate(units[s:s + blocks], axis=1) for s in range(0, ny, blocks)], axis=0
        )
        acc[g] += jnp.dot(hidden, dw_ref[layer, depth, :], preferred_element_type=F32)

    def settle(at, end, hop):
        for step in range(1, ny):
            y_copy(at, step).wait_send()

        @pl.when(hop < nz - 1)
        def _():
            z_copy(at, end).wait_send()

        @pl.when(hop == nz - 1)
        def _():
            for step in range(1, ny):
                hy_copy(at, step, me_y).wait_send()

        @pl.when(hop > 0)
        def _():
            hz_copy(at, end).wait_send()

    def half_of(which):
        return pl.ds(pl.multiple_of(which * half_rows, half_rows), half_rows)

    def core_sum(layer, g):
        c_out[layer, g] = acc[g, half_of(1 - core), :].astype(BF16)
        core_copy(layer, g).start()

    def chip_sum(layer, g):
        core_copy(layer, g).wait()
        value = acc[g, half_of(core), :] + c_in[layer, g].astype(F32)
        c_sum[layer, g, me_cb] = value.astype(BF16)
        for step in range(1, n_cb):
            sum_copy(layer, g, step, me_cb).start()

    def finish(layer, g):
        for step in range(1, n_cb):
            sum_copy(layer, g, step, lax.rem(me_cb - step + n_cb, n_cb)).wait_recv()
            sum_copy(layer, g, step, me_cb).wait_send()
        for c in range(CORES):
            branch = c_sum[layer, g, c].astype(F32)
            for chip in range(1, n_cb // CORES):
                branch = branch + c_sum[layer, g, chip * CORES + c].astype(F32)
            span = pl.ds(c * half_rows, half_rows)
            carried[g, span, :] = RESID * carried[g, span, :] + branch

        @pl.when(layer < layers - 1)
        def _():
            prepare(layer + 1, g)
            send_squares(layer + 1, g)

        @pl.when(layer == layers - 1)
        def _():
            out_ref[g] = carried[g].astype(out_ref.dtype)

    for g in range(groups):
        carried[g] = tok_ref[g].astype(F32)
        prepare(0, g)
    pl.semaphore_wait(barrier, n_ra + n_cb - 2)
    for g in range(groups):
        send_squares(0, g)

    act_lag = LAG_Y + LAG_Z * (nz - 1)
    gather_lag = act_lag + LAG_HY
    down_lag = gather_lag + LAG_HZ * (nz - 1)
    total_lag = down_lag + TAIL_END
    stride = max(per_layer, chunks + total_lag)

    def body(t, _):
        def place(lag):
            at = t - lag
            layer, q = lax.div(at, stride), lax.rem(at, stride)
            active = (at >= 0) & (q < per_layer) & (layer < layers)
            end = lax.rem(q, 2)
            hop = jnp.where(end == 0, nz - 1 - me_z, me_z)
            return active, layer, lax.div(q, chunks), lax.rem(q, chunks), layer * per_layer + q, end, hop

        active, layer, g, i, at, end, hop = place(down_lag + TAIL_END)

        @pl.when(active & (i == chunks - 1))
        def _():
            finish(layer, g)

        active, layer, g, i, at, end, hop = place(down_lag + TAIL_SUM)

        @pl.when(active & (i == chunks - 1))
        def _():
            chip_sum(layer, g)

        for far in range(nz - 2, 0, -1):
            active, layer, g, i, at, end, hop = place(gather_lag + LAG_HZ * far)

            @pl.when(active & (hop == nz - 1 - far))
            def _():
                hz_copy(at, end).wait_recv()
                hz_copy(at, end).start()

        active, layer, g, i, at, end, hop = place(gather_lag)

        @pl.when(active & (hop == nz - 1))
        def _():
            gather_y(at)
            hz_copy(at, end).start()

        active, layer, g, i, at, end, hop = place(act_lag)

        @pl.when(active & (i == 0))
        def _():
            scale(layer, g)

        @pl.when(active & (hop == nz - 1))
        def _():
            activate(layer, g, i, at, end)

        for k in range(nz - 2, 0, -1):
            active, layer, g, i, at, end, hop = place(LAG_Y + LAG_Z * k)

            @pl.when(active & (hop == k))
            def _():
                part[at, me_y] = add_z(at, end).astype(BF16)
                z_copy(at, end).start()

        active, layer, g, i, at, end, hop = place(LAG_Y)

        @pl.when(active)
        def _():
            add_y(at)

        @pl.when(active & (hop == 0))
        def _():
            z_copy(at, end).start()

        active, layer, g, i, at, end, hop = place(0)

        @pl.when(active)
        def _():
            project(layer, g, i, at)

        active, layer, g, i, at, end, hop = place(down_lag)

        @pl.when(active & (hop == 0))
        def _():
            hz_copy(at, end).wait_recv()

        @pl.when(active)
        def _():
            down(layer, g, i, at)
            settle(at, end, hop)

        @pl.when(active & (i == chunks - 1))
        def _():
            core_sum(layer, g)

        return 0

    lax.fori_loop(0, stride * (layers - 1) + per_layer + total_lag, body, 0)


def per_device(n_ra, n_cb, tokens, gain, gw, uw, gt, ut, gb, ub, dw):
    seqs, length, d = tokens.shape
    layers, _, ff = gw.shape
    nz = seqs
    ny = n_ra // nz
    blocks = ny if ff % (ny * LANES) == 0 else 1
    width = blocks * LANES
    groups = seqs * blocks // ny
    rows = seqs * length // groups
    chunks = ff // width
    n = layers * groups * chunks
    dims = (n_ra, n_cb, nz, groups, rows, length, layers, width, chunks)
    vmem = pl.BlockSpec(memory_space=pltpu.VMEM)
    hbm = pl.BlockSpec(memory_space=pl.ANY)
    dma = pltpu.SemaphoreType.DMA
    ys = max(ny - 1, 1)
    half = rows // CORES
    scratch = [
        pltpu.VMEM((layers, d, ff), BF16),
        pltpu.VMEM((layers, d, ff), BF16),
        pltpu.VMEM((layers, ff, d), BF16),
        pltpu.VMEM((groups, rows, d), F32),
        pltpu.VMEM((groups, rows, d), BF16),
        pltpu.VMEM((groups, rows, LANES), F32),
        pltpu.VMEM((groups, rows, d), F32),
        pltpu.VMEM((layers, groups, 1, rows), F32),
        pltpu.VMEM((layers, groups, n_ra - 1, 1, rows), F32),
        pltpu.VMEM((n, ny, length, 2 * LANES), BF16),
        pltpu.VMEM((n, ys, length, 2 * LANES), BF16),
        pltpu.VMEM((n, length, 2 * LANES), BF16),
        pltpu.VMEM((n, ny, length, LANES), BF16),
        pltpu.VMEM((layers, groups, half, d), BF16),
        pltpu.VMEM((layers, groups, half, d), BF16),
        pltpu.VMEM((layers, groups, n_cb, half, d), BF16),
        dma((layers, chunks, 3)),
        dma((layers, groups, n_ra - 1)), dma((layers, groups, n_ra - 1)),
        dma((n, ys)), dma((n, ys)),
        dma((n,)), dma((n,)),
        dma((n, ys)), dma((n, ys)),
        dma((n,)), dma((n,)),
        dma((layers, groups)), dma((layers, groups)),
        dma((layers, groups, n_cb - 1)), dma((layers, groups, n_cb - 1)),
    ]
    out = pl.pallas_call(
        functools.partial(kernel, dims),
        out_shape=jax.ShapeDtypeStruct((groups, rows, d), tokens.dtype),
        in_specs=[vmem, vmem, hbm, hbm, vmem, vmem, vmem, vmem, hbm],
        out_specs=vmem,
        scratch_shapes=scratch,
        compiler_params=pltpu.CompilerParams(
            collective_id=0, has_side_effects=True, vmem_limit_bytes=60 * 1024 * 1024
        ),
        name="blocks",
    )(
        tokens.reshape(groups, rows, d), gain[:, None, :], gw, uw, gt, ut,
        gb[:, None, :], ub[:, None, :], dw,
    )
    return out.reshape(tokens.shape)


def solution(mesh):
    in_specs = (
        P(None, None, "ra"),
        P(None, "ra"),
        P(None, "ra", "cb"),
        P(None, "ra", "cb"),
        P(None, None, "cb"),
        P(None, None, "cb"),
        P(None, "cb"),
        P(None, "cb"),
        P(None, "cb", "ra"),
    )
    return jax.shard_map(
        functools.partial(per_device, mesh.shape["ra"], mesh.shape["cb"]),
        mesh=mesh, in_specs=in_specs, out_specs=P(None, None, "ra"), check_vma=False,
    )
```

time: 231 us -> 232 us (level)
  no operation moved by 1% of the time
where the time goes in v1:
time: 232 us
  Pallas kernels  223 us (96%)
  local copies, waits for them, and re-layouts  8.92 us (4%)
    pallas_call x1, Pallas kernels, per_device(): pl.pallas_call(functools.partial(kernel, dims), out_shape=jax.ShapeDtypeS...  223 us
    unnamed x3, local copies, waits for them, and re-layouts  4.95 us

profile of v1, /device:TPU:0, one launch (start us, length us, event | category | flops | bytes accessed | tf_op | source)
XLA Modules:
  0.0 231.5 jit_solution(18045062203789348994)
XLA Ops:
  0.0 1.3 broadcast_in_dim.9.gain_ref
  1.3 1.4 broadcast_in_dim.10.gb_ref
  2.6 1.3 broadcast_in_dim.11.ub_ref
  4.0 1.5 copy.10.gt_ref
  5.5 1.5 copy.11.ut_ref
  7.1 222.6 %blocks.1 = bf16[4,128,512]{2,1,0:T(8,128)(2,1)} custom-call(bf16[4,128,512]{2,1,0:T(8,128)(2,1)} %tok_ref.1, f32[2,1,512]{2,1,0:T(1,128)} %broadcast_in_dim.9.gain_ref, bf16[2,512,2816]{2,1,0:T(8,128)(2,1)} %gw_hbm.1, bf16[2,512,2816]{2,1,0:T(8,128)(2,1)} %uw_hbm.1, f32[2,3,2816]{2,1,0:T(4,128)} %copy.10.gt_ref, f32[2,3,2816]{2,1,0:T(4,128)} %copy.11.ut_ref, ...), custom_call_target="tpu_custom_call" | custom-call | tf_op jit(solution)/shard_map/blocks/pallas_call | solution.py:402
  229.7 1.9 copy.13

commit v2 on v1

--- a/solution.py
+++ b/solution.py
@@ -11,8 +11,9 @@
 RESID = 0.5
 LANES = 128
 CORES = 2
-LAG_Y, LAG_Z, LAG_HY, LAG_HZ = 2, 2, 2, 2
-TAIL_SUM, TAIL_END = 1, 4
+LAG_Y, LAG_Z, LAG_HY, LAG_HZ = 4, 4, 4, 4
+TAIL_CHIP, TAIL_SUM, TAIL_END = 1, 4, 5
+SPLIT, SPREAD = 1 / 2, 1 / 2
 
 MESH = pl.DeviceIdType.MESH
 F32, BF16 = jnp.float32, jnp.bfloat16
@@ -23,8 +24,8 @@
     tok_ref, gain_ref, gw_hbm, uw_hbm, gt_ref, ut_ref, gb_ref, ub_ref, dw_hbm,
     out_ref,
     gw_ref, uw_ref, dw_ref, carried, scaled, inv, acc,
-    sq_own, sq_in, part, y_in, z_in, hid, c_out, c_in, c_sum,
-    w_sem, sq_s, sq_r, y_s, y_r, z_s, z_r, hy_s, hy_r, hz_s, hz_r, c_s, c_r, ca_s, ca_r,
+    sq_own, sq_in, part, y_in, z_in, hid, c_out, c_in, c_sum, c_all,
+    w_sem, sq_s, sq_r, y_s, y_r, z_s, z_r, wz_s, wz_r, wy_s, wy_r, hy_s, hy_r, hz_s, hz_r, nz_s, nz_r, ny_s, ny_r, c_s, c_r, cs_s, cs_r, ca_s, ca_r,
 ):
     n_ra, n_cb, nz, groups, rows, length, layers, width, chunks = dims
     ny = n_ra // nz
@@ -34,7 +35,7 @@
     me_ra = lax.axis_index("ra")
     me_cb = lax.axis_index("cb")
     me_z, me_y = me_ra // ny, me_ra % ny
-    core = me_cb % CORES
+    core, chip, chips = me_cb % CORES, me_cb // CORES, n_cb // CORES
     seq, block = me_y // blocks, me_y % blocks
 
     def weight_copies(layer, i):
@@ -82,18 +83,36 @@
             ra=lax.rem(me_ra + step, n_ra),
         )
 
+    split = int(length * SPLIT) // 16 * 16
+    first, rest = pl.ds(0, split), pl.ds(split, length - split)
+
     def y_copy(at, step):
         to = lax.rem(me_y + step, ny)
         return remote(
-            part.at[at, to], y_in.at[at, step - 1],
+            part.at[at, to, first], y_in.at[at, step - 1, first],
             y_s.at[at, step - 1], y_r.at[at, step - 1], ra=me_z * ny + to,
+        )
+
+    def late_copy(at, step):
+        to = lax.rem(me_y + step, ny)
+        return remote(
+            part.at[at, to, rest], y_in.at[at, step - 1, rest],
+            wy_s.at[at, step - 1], wy_r.at[at, step - 1], ra=me_z * ny + to,
         )
 
     def along(end):
         return lax.rem(me_z + 2 * end - 1 + nz, nz) * ny + me_y
 
     def z_copy(at, end):
-        return remote(part.at[at, me_y], z_in.at[at], z_s.at[at], z_r.at[at], ra=along(end))
+        return remote(
+            part.at[at, me_y, first], z_in.at[at, 0, first], z_s.at[at], z_r.at[at],
+            ra=along(end),
+        )
+
+    def wide_copy(at, end):
+        return remote(
+            part.at[at, :, rest], z_in.at[at, :, rest], wz_s.at[at], wz_r.at[at], ra=along(end)
+        )
 
     def hy_copy(at, step, y):
         to = lax.rem(me_y + step, ny)
@@ -102,8 +121,23 @@
             block, block, hy_s.at[at, step - 1], hy_r.at[at, step - 1], ra=me_z * ny + to
         )
 
+    spread = int(length * SPREAD) // 16 * 16
+    both, own = pl.ds(0, spread), pl.ds(spread, length - spread)
+
     def hz_copy(at, end):
-        return remote(hid.at[at], hid.at[at], hz_s.at[at], hz_r.at[at], ra=along(1 - end))
+        rows_of = hid.at[at, :, both]
+        return remote(rows_of, rows_of, hz_s.at[at], hz_r.at[at], ra=along(1 - end))
+
+    def own_copy(at, end):
+        rows_of = hid.at[at, me_y, own]
+        return remote(rows_of, rows_of, nz_s.at[at], nz_r.at[at], ra=along(1 - end))
+
+    def cross_copy(at, step, y):
+        rows_of = hid.at[at, y, own]
+        return remote(
+            rows_of, rows_of, ny_s.at[at, step - 1], ny_r.at[at, step - 1],
+            ra=me_z * ny + lax.rem(me_y + step, ny),
+        )
 
     def core_copy(layer, g):
         return remote(
@@ -111,20 +145,32 @@
             cb=me_cb + 1 - 2 * core,
         )
 
-    def sum_copy(layer, g, step, block):
-        to = lax.rem(me_cb + step, n_cb)
-        block = c_sum.at[layer, g, block]
-        return remote(
-            block, block, ca_s.at[layer, g, step - 1], ca_r.at[layer, g, step - 1], cb=to
+    def sum_copy(layer, g, step, source):
+        piece = c_sum.at[layer, g, source]
+        return remote(
+            piece, piece, cs_s.at[layer, g, step - 1], cs_r.at[layer, g, step - 1],
+            cb=lax.rem(chip + step, chips) * CORES + core,
+        )
+
+    def all_copy(layer, g, source):
+        piece = c_all.at[layer, g, source]
+        return remote(
+            piece, piece, ca_s.at[layer, g], ca_r.at[layer, g], cb=me_cb + 1 - 2 * core
         )
 
     row_in_seq = lax.broadcasted_iota(jnp.int32, (length, LANES), 0)
+
+    def of_layer(values, layer):
+        picked = values[:1]
+        for other in range(1, layers):
+            picked = jnp.where(layer == other, values[other:other + 1], picked)
+        return picked
 
     def prepare(layer, g):
         values = carried[g]
         squares = jnp.sum(values * values, axis=1, keepdims=True)
         sq_own[layer, g] = jnp.transpose(jnp.broadcast_to(squares, (rows, LANES)))[:1]
-        scaled[g] = (values * gain_ref[layer]).astype(BF16)
+        scaled[g] = (values * of_layer(gain_ref[...], layer)).astype(BF16)
         acc[g] = jnp.zeros(acc.shape[1:], F32)
 
     def send_squares(layer, g):
@@ -137,9 +183,9 @@
             square_copy(layer, g, step).wait()
             total = total + sq_in[layer, g, step - 1]
         total = jnp.transpose(jnp.broadcast_to(total, (LANES, rows)))
-        inv[g] = lax.rsqrt(total / (n_ra * gain_ref.shape[2]) + EPS)
-
-    def project(layer, g, i, at):
+        inv[g] = lax.rsqrt(total / (n_ra * gain_ref.shape[1]) + EPS)
+
+    def project(layer, g, i, at, end, hop):
         @pl.when(g == 0)
         def _():
             for copy in weight_copies(layer, i)[:2]:
@@ -153,22 +199,33 @@
                 part[at, unit, :, half * LANES:(half + 1) * LANES] = product[
                     s * length:(s + 1) * length, b * LANES:(b + 1) * LANES
                 ].astype(BF16)
+
         for step in range(1, ny):
             y_copy(at, step).start()
 
-    def add_y(at):
-        value = part[at, me_y].astype(F32)
+        @pl.when(hop == 0)
+        def _():
+            wide_copy(at, end).start()
+
+    def add_y(at, copy, span):
+        value = part[at, me_y, span].astype(F32)
         for step in range(1, ny):
-            y_copy(at, step).wait_recv()
-            value = value + y_in[at, step - 1].astype(F32)
-        part[at, me_y] = value.astype(BF16)
+            copy(at, step).wait_recv()
+            value = value + y_in[at, step - 1, span].astype(F32)
+        return value
 
     def add_z(at, end):
         z_copy(at, end).wait_recv()
-        return part[at, me_y].astype(F32) + z_in[at].astype(F32)
+        return part[at, me_y, first].astype(F32) + z_in[at, 0, first].astype(F32)
+
+    def add_wide(at, end):
+        wide_copy(at, end).wait_recv()
+        for unit in range(ny):
+            total = part[at, unit, rest].astype(F32) + z_in[at, unit, rest].astype(F32)
+            part[at, unit, rest] = total.astype(BF16)
 
     def activate(layer, g, i, at, end):
-        value = add_z(at, end)
+        value = jnp.concatenate([add_z(at, end), add_y(at, late_copy, rest)], axis=0)
         cols = pl.ds(pl.multiple_of(i * width + block * LANES, LANES), LANES)
         factor = inv[g, pl.ds(pl.multiple_of(seq * length, length), length), :]
         conv = []
@@ -177,14 +234,15 @@
             pre = pre.astype(BF16).astype(F32)
             last = jnp.where(row_in_seq >= 1, pltpu.roll(pre, 1, 0), 0.0)
             older = jnp.where(row_in_seq >= 2, pltpu.roll(pre, 2, 0), 0.0)
-            tap = [taps[layer, pl.ds(k, 1), cols] for k in range(3)]
+            tap = [of_layer(taps[k, :, cols], layer) for k in range(3)]
             conv.append(
-                bias[layer, :, cols] + tap[0] * older + tap[1] * last + tap[2] * pre
+                of_layer(bias[:, cols], layer) + tap[0] * older + tap[1] * last + tap[2] * pre
             )
         gate, up = conv
         hid[at, me_y] = (gate / (1.0 + jnp.exp(-gate)) * up).astype(BF16)
         for step in range(1, ny):
             hy_copy(at, step, me_y).start()
+        own_copy(at, end).start()
 
     def gather_y(at):
         for step in range(1, ny):
@@ -209,15 +267,23 @@
         @pl.when(hop < nz - 1)
         def _():
             z_copy(at, end).wait_send()
+            wide_copy(at, end).wait_send()
 
         @pl.when(hop == nz - 1)
         def _():
             for step in range(1, ny):
+                late_copy(at, step).wait_send()
                 hy_copy(at, step, me_y).wait_send()
 
         @pl.when(hop > 0)
         def _():
             hz_copy(at, end).wait_send()
+            own_copy(at, end).wait_send()
+
+        @pl.when(hop < nz - 1)
+        def _():
+            for step in range(1, ny):
+                cross_copy(at, step, me_y).wait_send()
 
     def half_of(which):
         return pl.ds(pl.multiple_of(which * half_rows, half_rows), half_rows)
@@ -229,20 +295,25 @@
     def chip_sum(layer, g):
         core_copy(layer, g).wait()
         value = acc[g, half_of(core), :] + c_in[layer, g].astype(F32)
-        c_sum[layer, g, me_cb] = value.astype(BF16)
-        for step in range(1, n_cb):
-            sum_copy(layer, g, step, me_cb).start()
+        c_sum[layer, g, chip] = value.astype(BF16)
+        for step in range(1, chips):
+            sum_copy(layer, g, step, chip).start()
+
+    def total_sum(layer, g):
+        for step in range(1, chips):
+            sum_copy(layer, g, step, lax.rem(chip - step + chips, chips)).wait_recv()
+            sum_copy(layer, g, step, chip).wait_send()
+        value = c_sum[layer, g, 0].astype(F32)
+        for other in range(1, chips):
+            value = value + c_sum[layer, g, other].astype(F32)
+        c_all[layer, g, core] = value.astype(BF16)
+        all_copy(layer, g, core).start()
 
     def finish(layer, g):
-        for step in range(1, n_cb):
-            sum_copy(layer, g, step, lax.rem(me_cb - step + n_cb, n_cb)).wait_recv()
-            sum_copy(layer, g, step, me_cb).wait_send()
-        for c in range(CORES):
-            branch = c_sum[layer, g, c].astype(F32)
-            for chip in range(1, n_cb // CORES):
-                branch = branch + c_sum[layer, g, chip * CORES + c].astype(F32)
-            span = pl.ds(c * half_rows, half_rows)
-            carried[g, span, :] = RESID * carried[g, span, :] + branch
+        all_copy(layer, g, 1 - core).wait_recv()
+        all_copy(layer, g, core).wait_send()
+        branch = c_all[layer, g].reshape(rows, c_all.shape[4]).astype(F32)
+        carried[g] = RESID * carried[g] + branch
 
         @pl.when(layer < layers - 1)
         def _():
@@ -253,12 +324,13 @@
         def _():
             out_ref[g] = carried[g].astype(out_ref.dtype)
 
-    for g in range(groups):
+    def enter(g):
         carried[g] = tok_ref[g].astype(F32)
         prepare(0, g)
+
+    enter(0)
     pl.semaphore_wait(barrier, n_ra + n_cb - 2)
-    for g in range(groups):
-        send_squares(0, g)
+    send_squares(0, 0)
 
     act_lag = LAG_Y + LAG_Z * (nz - 1)
     gather_lag = act_lag + LAG_HY
@@ -273,19 +345,26 @@
             active = (at >= 0) & (q < per_layer) & (layer < layers)
             end = lax.rem(q, 2)
             hop = jnp.where(end == 0, nz - 1 - me_z, me_z)
-            return active, layer, lax.div(q, chunks), lax.rem(q, chunks), layer * per_layer + q, end, hop
-
-        active, layer, g, i, at, end, hop = place(down_lag + TAIL_END)
-
-        @pl.when(active & (i == chunks - 1))
-        def _():
-            finish(layer, g)
-
-        active, layer, g, i, at, end, hop = place(down_lag + TAIL_SUM)
-
-        @pl.when(active & (i == chunks - 1))
-        def _():
-            chip_sum(layer, g)
+            spot = lax.div(q, chunks), lax.rem(q, chunks), layer * per_layer + q
+            return active, layer, *spot, end, hop
+
+        for lag, stage in ((TAIL_END, finish), (TAIL_SUM, total_sum), (TAIL_CHIP, chip_sum)):
+            active, layer, g, i, at, end, hop = place(down_lag + lag)
+
+            @pl.when(active & (i == chunks - 1))
+            def _():
+                stage(layer, g)
+
+        for far in range(nz - 1, 0, -1):
+            active, layer, g, i, at, end, hop = place(act_lag + LAG_HZ * far)
+
+            @pl.when(active & (hop == nz - 1 - far))
+            def _():
+                own_copy(at, end).wait_recv()
+                if far < nz - 1:
+                    own_copy(at, end).start()
+                for step in range(1, ny):
+                    cross_copy(at, step, me_y).start()
 
         for far in range(nz - 2, 0, -1):
             active, layer, g, i, at, end, hop = place(gather_lag + LAG_HZ * far)
@@ -312,19 +391,34 @@
         def _():
             activate(layer, g, i, at, end)
 
+        active, layer, g, i, at, end, hop = place(LAG_Z * (nz - 1))
+
+        @pl.when(active & (hop == nz - 1))
+        def _():
+            add_wide(at, end)
+            for step in range(1, ny):
+                late_copy(at, step).start()
+
         for k in range(nz - 2, 0, -1):
-            active, layer, g, i, at, end, hop = place(LAG_Y + LAG_Z * k)
+            active, layer, g, i, at, end, hop = place(LAG_Z * k)
 
             @pl.when(active & (hop == k))
             def _():
-                part[at, me_y] = add_z(at, end).astype(BF16)
+                add_wide(at, end)
+                wide_copy(at, end).start()
+
+            active, layer, g, i, at, end, hop = place(LAG_Y + LAG_Z * k)
+
+            @pl.when(active & (hop == k))
+            def _():
+                part[at, me_y, first] = add_z(at, end).astype(BF16)
                 z_copy(at, end).start()
 
         active, layer, g, i, at, end, hop = place(LAG_Y)
 
         @pl.when(active)
         def _():
-            add_y(at)
+            part[at, me_y, first] = add_y(at, y_copy, first).astype(BF16)
 
         @pl.when(active & (hop == 0))
         def _():
@@ -332,15 +426,25 @@
 
         active, layer, g, i, at, end, hop = place(0)
 
+        @pl.when(active & (layer == 0) & (i == 0) & (g > 0))
+        def _():
+            enter(g)
+            send_squares(0, g)
+
         @pl.when(active)
         def _():
-            project(layer, g, i, at)
+            project(layer, g, i, at, end, hop)
 
         active, layer, g, i, at, end, hop = place(down_lag)
 
         @pl.when(active & (hop == 0))
         def _():
             hz_copy(at, end).wait_recv()
+
+        @pl.when(active & (hop < nz - 1))
+        def _():
+            for step in range(1, ny):
+                cross_copy(at, step, lax.rem(me_y - step + ny, ny)).wait_recv()
 
         @pl.when(active)
         def _():
@@ -372,7 +476,7 @@
     hbm = pl.BlockSpec(memory_space=pl.ANY)
     dma = pltpu.SemaphoreType.DMA
     ys = max(ny - 1, 1)
-    half = rows // CORES
+    half, chips = rows // CORES, n_cb // CORES
     scratch = [
         pltpu.VMEM((layers, d, ff), BF16),
         pltpu.VMEM((layers, d, ff), BF16),
@@ -385,19 +489,25 @@
         pltpu.VMEM((layers, groups, n_ra - 1, 1, rows), F32),
         pltpu.VMEM((n, ny, length, 2 * LANES), BF16),
         pltpu.VMEM((n, ys, length, 2 * LANES), BF16),
-        pltpu.VMEM((n, length, 2 * LANES), BF16),
+        pltpu.VMEM((n, ny, length, 2 * LANES), BF16),
         pltpu.VMEM((n, ny, length, LANES), BF16),
         pltpu.VMEM((layers, groups, half, d), BF16),
         pltpu.VMEM((layers, groups, half, d), BF16),
-        pltpu.VMEM((layers, groups, n_cb, half, d), BF16),
+        pltpu.VMEM((layers, groups, chips, half, d), BF16),
+        pltpu.VMEM((layers, groups, CORES, half, d), BF16),
         dma((layers, chunks, 3)),
         dma((layers, groups, n_ra - 1)), dma((layers, groups, n_ra - 1)),
         dma((n, ys)), dma((n, ys)),
         dma((n,)), dma((n,)),
+        dma((n,)), dma((n,)),
+        dma((n, ys)), dma((n, ys)),
         dma((n, ys)), dma((n, ys)),
         dma((n,)), dma((n,)),
+        dma((n,)), dma((n,)),
+        dma((n, ys)), dma((n, ys)),
         dma((layers, groups)), dma((layers, groups)),
-        dma((layers, groups, n_cb - 1)), dma((layers, groups, n_cb - 1)),
+        dma((layers, groups, max(chips - 1, 1))), dma((layers, groups, max(chips - 1, 1))),
+        dma((layers, groups)), dma((layers, groups)),
     ]
     out = pl.pallas_call(
         functools.partial(kernel, dims),
@@ -410,8 +520,8 @@
         ),
         name="blocks",
     )(
-        tokens.reshape(groups, rows, d), gain[:, None, :], gw, uw, gt, ut,
-        gb[:, None, :], ub[:, None, :], dw,
+        tokens.reshape(groups, rows, d), gain, gw, uw,
+        jnp.transpose(gt, (1, 0, 2)), jnp.transpose(ut, (1, 0, 2)), gb, ub, dw,
     )
     return out.reshape(tokens.shape)
 

time: 232 us -> 191 us (0.82)
  Pallas kernels: 223 us -> 189 us
  local copies, waits for them, and re-layouts: 8.92 us -> 1.87 us
    pallas_call x1, Pallas kernels: 223 us -> 189 us  [per_device(): pl.pallas_call(functools.partial(kernel, dims), out_shape=jax.ShapeDtypeS...]
    broadcast_in_dim x3 -> x0, local copies, waits for them, and re-layouts: 3.97 us -> none  [the longest x1 1.35 us: per_device(): gb[:, None, :]]
    unnamed x3 -> x1, local copies, waits for them, and re-layouts: 4.95 us -> 1.87 us
where the time goes in v2:
time: 191 us; the launch traced here: 190 us
  Pallas kernels  189 us (99%)
    pallas_call x1, Pallas kernels, per_device(): pl.pallas_call(functools.partial(kernel, dims), out_shape=jax.ShapeDtypeS...  189 us

profile of v2, /device:TPU:0, one launch (start us, length us, event | category | flops | bytes accessed | tf_op | source)
XLA Modules:
  0.0 190.4 jit_solution(2267621680470187624)
XLA Ops:
  0.0 188.6 %blocks.1 = bf16[4,128,512]{2,1,0:T(8,128)(2,1)} custom-call(bf16[4,128,512]{2,1,0:T(8,128)(2,1)} %tok_ref.1, f32[2,512]{1,0:T(2,128)} %gain_ref.1, bf16[2,512,2816]{2,1,0:T(8,128)(2,1)} %gw_hbm.1, bf16[2,512,2816]{2,1,0:T(8,128)(2,1)} %uw_hbm.1, f32[3,2,2816]{2,1,0:T(2,128)} %bitcast.2, f32[3,2,2816]{2,1,0:T(2,128)} %bitcast.3, f32[2,2816]{1,0:T(2,128)} %gb_ref.1, ...), custom_call_target="tpu_custom_call" | custom-call | tf_op jit(solution)/shard_map/blocks/pallas_call | solution.py:512
  188.6 1.9 copy.11

commit v3 on v2

--- a/solution.py
+++ b/solution.py
@@ -21,11 +21,12 @@
 
 def kernel(
     dims,
-    tok_ref, gain_ref, gw_hbm, uw_hbm, gt_ref, ut_ref, gb_ref, ub_ref, dw_hbm,
+    tok_hbm, gain_hbm, gw_hbm, uw_hbm, gt_hbm, ut_hbm, gb_hbm, ub_hbm, dw_hbm,
     out_ref,
+    tok_ref, gain_ref, gt_ref, ut_ref, gb_ref, ub_ref,
     gw_ref, uw_ref, dw_ref, carried, scaled, inv, acc,
-    sq_own, sq_in, part, y_in, z_in, hid, c_out, c_in, c_sum, c_all,
-    w_sem, sq_s, sq_r, y_s, y_r, z_s, z_r, wz_s, wz_r, wy_s, wy_r, hy_s, hy_r, hz_s, hz_r, nz_s, nz_r, ny_s, ny_r, c_s, c_r, cs_s, cs_r, ca_s, ca_r,
+    sq_own, sq_y, sq_sum, sq_fwd, sq_z, part, y_in, z_in, hid, c_out, c_in, c_sum, c_all,
+    i_sem, w_sem, sq_s, sq_r, sz_s, sz_r, y_s, y_r, z_s, z_r, wz_s, wz_r, wy_s, wy_r, hy_s, hy_r, hz_s, hz_r, nz_s, nz_r, ny_s, ny_r, c_s, c_r, cs_s, cs_r, ca_s, ca_r,
 ):
     n_ra, n_cb, nz, groups, rows, length, layers, width, chunks = dims
     ny = n_ra // nz
@@ -52,6 +53,36 @@
             ),
         ]
 
+    barrier = pltpu.get_barrier_semaphore()
+    def greet(**where):
+        pl.semaphore_signal(barrier, inc=1, device_id=where, device_id_type=MESH)
+
+    for step in range(1, ny):
+        greet(ra=me_z * ny + lax.rem(me_y + step, ny))
+    for step in range(1, chips):
+        greet(cb=lax.rem(chip + step, chips) * CORES + core)
+    greet(cb=me_cb + 1 - 2 * core)
+
+    @pl.when(me_z > 0)
+    def _():
+        greet(ra=me_ra - ny)
+
+    @pl.when(me_z < nz - 1)
+    def _():
+        greet(ra=me_ra + ny)
+
+    guests = ny + chips - 1 + jnp.where(me_z > 0, 1, 0) + jnp.where(me_z < nz - 1, 1, 0)
+
+    inputs = [
+        pltpu.make_async_copy(source, target, i_sem.at[k])
+        for k, (source, target) in enumerate((
+            (tok_hbm, tok_ref), (gain_hbm, gain_ref), (gt_hbm, gt_ref), (ut_hbm, ut_ref),
+            (gb_hbm, gb_ref), (ub_hbm, ub_ref),
+        ))
+    ]
+    for copy in inputs:
+        copy.start()
+
     for layer in range(layers):
         def fetch(i, _, layer=layer):
             for copy in weight_copies(layer, i):
@@ -60,16 +91,6 @@
 
         lax.fori_loop(0, chunks, fetch, 0)
 
-    barrier = pltpu.get_barrier_semaphore()
-    for step in range(1, n_ra):
-        pl.semaphore_signal(
-            barrier, inc=1, device_id={"ra": lax.rem(me_ra + step, n_ra)}, device_id_type=MESH
-        )
-    for step in range(1, n_cb):
-        pl.semaphore_signal(
-            barrier, inc=1, device_id={"cb": lax.rem(me_cb + step, n_cb)}, device_id_type=MESH
-        )
-
     def remote(src, dst, send, recv, **where):
         return pltpu.make_async_remote_copy(
             src_ref=src, dst_ref=dst, send_sem=send, recv_sem=recv,
@@ -78,9 +99,15 @@
 
     def square_copy(layer, g, step):
         return remote(
-            sq_own.at[layer, g], sq_in.at[layer, g, step - 1],
+            sq_own.at[layer, g], sq_y.at[layer, g, step - 1],
             sq_s.at[layer, g, step - 1], sq_r.at[layer, g, step - 1],
-            ra=lax.rem(me_ra + step, n_ra),
+            ra=me_z * ny + lax.rem(me_y + step, ny),
+        )
+
+    def square_along(layer, g, end):
+        return remote(
+            sq_fwd.at[layer, g, end], sq_z.at[layer, g, end],
+            sz_s.at[layer, g, end], sz_r.at[layer, g, end], ra=along(end),
         )
 
     split = int(length * SPLIT) // 16 * 16
@@ -174,16 +201,36 @@
         acc[g] = jnp.zeros(acc.shape[1:], F32)
 
     def send_squares(layer, g):
-        for step in range(1, n_ra):
+        for step in range(1, ny):
             square_copy(layer, g, step).start()
 
-    def scale(layer, g):
+    def add_squares(layer, g):
         total = sq_own[layer, g]
-        for step in range(1, n_ra):
-            square_copy(layer, g, step).wait()
-            total = total + sq_in[layer, g, step - 1]
+        for step in range(1, ny):
+            square_copy(layer, g, step).wait_recv()
+            total = total + sq_y[layer, g, step - 1]
+        sq_sum[layer, g] = total
+
+    def chain_squares(layer, g, end):
+        square_along(layer, g, end).wait_recv()
+        return sq_sum[layer, g] + sq_z[layer, g, end]
+
+    def scale(layer, g, end):
+        total = chain_squares(layer, g, end)
         total = jnp.transpose(jnp.broadcast_to(total, (LANES, rows)))
         inv[g] = lax.rsqrt(total / (n_ra * gain_ref.shape[1]) + EPS)
+
+    def settle_squares(layer, g):
+        for step in range(1, ny):
+            square_copy(layer, g, step).wait_send()
+
+        @pl.when(me_z > 0)
+        def _():
+            square_along(layer, g, 0).wait_send()
+
+        @pl.when(me_z < nz - 1)
+        def _():
+            square_along(layer, g, 1).wait_send()
 
     def project(layer, g, i, at, end, hop):
         @pl.when(g == 0)
@@ -312,6 +359,7 @@
     def finish(layer, g):
         all_copy(layer, g, 1 - core).wait_recv()
         all_copy(layer, g, core).wait_send()
+        settle_squares(layer, g)
         branch = c_all[layer, g].reshape(rows, c_all.shape[4]).astype(F32)
         carried[g] = RESID * carried[g] + branch
 
@@ -328,8 +376,10 @@
         carried[g] = tok_ref[g].astype(F32)
         prepare(0, g)
 
+    for copy in inputs:
+        copy.wait()
     enter(0)
-    pl.semaphore_wait(barrier, n_ra + n_cb - 2)
+    pl.semaphore_wait(barrier, guests)
     send_squares(0, 0)
 
     act_lag = LAG_Y + LAG_Z * (nz - 1)
@@ -337,26 +387,54 @@
     down_lag = gather_lag + LAG_HZ * (nz - 1)
     total_lag = down_lag + TAIL_END
     stride = max(per_layer, chunks + total_lag)
+    stride += stride % 2
+    gap = stride - per_layer
 
     def body(t, _):
+        odd = lax.rem(t, 2)
+        towards = odd, 1 - odd
+        hops = [jnp.where(end == 0, nz - 1 - me_z, me_z) for end in towards]
+
         def place(lag):
-            at = t - lag
-            layer, q = lax.div(at, stride), lax.rem(at, stride)
-            active = (at >= 0) & (q < per_layer) & (layer < layers)
-            end = lax.rem(q, 2)
-            hop = jnp.where(end == 0, nz - 1 - me_z, me_z)
-            spot = lax.div(q, chunks), lax.rem(q, chunks), layer * per_layer + q
-            return active, layer, *spot, end, hop
+            spot = t - lag
+            layer = 0
+            for other in range(1, layers):
+                layer = layer + jnp.where(spot >= other * stride, 1, 0)
+            at = spot - layer * gap
+            active = (spot >= 0) & (at < (layer + 1) * per_layer)
+            return active, at, towards[lag % 2], hops[lag % 2], layer
+
+        def split_up(at, layer):
+            q = at - layer * per_layer
+            g = lax.div(q, chunks)
+            return g, q - g * chunks
 
         for lag, stage in ((TAIL_END, finish), (TAIL_SUM, total_sum), (TAIL_CHIP, chip_sum)):
-            active, layer, g, i, at, end, hop = place(down_lag + lag)
-
-            @pl.when(active & (i == chunks - 1))
-            def _():
-                stage(layer, g)
+            active, at, end, hop, layer = place(down_lag + lag)
+
+            @pl.when(active)
+            def _():
+                g, i = split_up(at, layer)
+
+                @pl.when(i == chunks - 1)
+                def _():
+                    stage(layer, g)
+
+        active, at, end, hop, layer = place(0)
+
+        @pl.when(active)
+        def _():
+            g, i = split_up(at, layer)
+
+            @pl.when((layer == 0) & (i == 0) & (g > 0))
+            def _():
+                enter(g)
+                send_squares(0, g)
+
+            project(layer, g, i, at, end, hop)
 
         for far in range(nz - 1, 0, -1):
-            active, layer, g, i, at, end, hop = place(act_lag + LAG_HZ * far)
+            active, at, end, hop, layer = place(act_lag + LAG_HZ * far)
 
             @pl.when(active & (hop == nz - 1 - far))
             def _():
@@ -367,31 +445,35 @@
                     cross_copy(at, step, me_y).start()
 
         for far in range(nz - 2, 0, -1):
-            active, layer, g, i, at, end, hop = place(gather_lag + LAG_HZ * far)
+            active, at, end, hop, layer = place(gather_lag + LAG_HZ * far)
 
             @pl.when(active & (hop == nz - 1 - far))
             def _():
                 hz_copy(at, end).wait_recv()
                 hz_copy(at, end).start()
 
-        active, layer, g, i, at, end, hop = place(gather_lag)
+        active, at, end, hop, layer = place(gather_lag)
 
         @pl.when(active & (hop == nz - 1))
         def _():
             gather_y(at)
             hz_copy(at, end).start()
 
-        active, layer, g, i, at, end, hop = place(act_lag)
-
-        @pl.when(active & (i == 0))
-        def _():
-            scale(layer, g)
-
-        @pl.when(active & (hop == nz - 1))
-        def _():
-            activate(layer, g, i, at, end)
-
-        active, layer, g, i, at, end, hop = place(LAG_Z * (nz - 1))
+        active, at, end, hop, layer = place(act_lag)
+
+        @pl.when(active)
+        def _():
+            g, i = split_up(at, layer)
+
+            @pl.when((i < 2) & (hop == nz - 1))
+            def _():
+                scale(layer, g, end)
+
+            @pl.when(hop == nz - 1)
+            def _():
+                activate(layer, g, i, at, end)
+
+        active, at, end, hop, layer = place(LAG_Z * (nz - 1))
 
         @pl.when(active & (hop == nz - 1))
         def _():
@@ -400,60 +482,68 @@
                 late_copy(at, step).start()
 
         for k in range(nz - 2, 0, -1):
-            active, layer, g, i, at, end, hop = place(LAG_Z * k)
+            active, at, end, hop, layer = place(LAG_Z * k)
 
             @pl.when(active & (hop == k))
             def _():
                 add_wide(at, end)
                 wide_copy(at, end).start()
 
-            active, layer, g, i, at, end, hop = place(LAG_Y + LAG_Z * k)
+            active, at, end, hop, layer = place(LAG_Y + LAG_Z * k)
 
             @pl.when(active & (hop == k))
             def _():
                 part[at, me_y, first] = add_z(at, end).astype(BF16)
                 z_copy(at, end).start()
-
-        active, layer, g, i, at, end, hop = place(LAG_Y)
+                g, i = split_up(at, layer)
+
+                @pl.when(i < 2)
+                def _():
+                    sq_fwd[layer, g, end] = chain_squares(layer, g, end)
+                    square_along(layer, g, end).start()
+
+        active, at, end, hop, layer = place(LAG_Y)
 
         @pl.when(active)
         def _():
             part[at, me_y, first] = add_y(at, y_copy, first).astype(BF16)
 
-        @pl.when(active & (hop == 0))
-        def _():
-            z_copy(at, end).start()
-
-        active, layer, g, i, at, end, hop = place(0)
-
-        @pl.when(active & (layer == 0) & (i == 0) & (g > 0))
-        def _():
-            enter(g)
-            send_squares(0, g)
+            @pl.when(hop == 0)
+            def _():
+                z_copy(at, end).start()
+
+            g, i = split_up(at, layer)
+
+            @pl.when(i == 0)
+            def _():
+                add_squares(layer, g)
+
+            @pl.when((i < 2) & (hop == 0))
+            def _():
+                sq_fwd[layer, g, end] = sq_sum[layer, g]
+                square_along(layer, g, end).start()
+
+        active, at, end, hop, layer = place(down_lag)
 
         @pl.when(active)
         def _():
-            project(layer, g, i, at, end, hop)
-
-        active, layer, g, i, at, end, hop = place(down_lag)
-
-        @pl.when(active & (hop == 0))
-        def _():
-            hz_copy(at, end).wait_recv()
-
-        @pl.when(active & (hop < nz - 1))
-        def _():
-            for step in range(1, ny):
-                cross_copy(at, step, lax.rem(me_y - step + ny, ny)).wait_recv()
-
-        @pl.when(active)
-        def _():
+            g, i = split_up(at, layer)
+
+            @pl.when(hop == 0)
+            def _():
+                hz_copy(at, end).wait_recv()
+
+            @pl.when(hop < nz - 1)
+            def _():
+                for step in range(1, ny):
+                    cross_copy(at, step, lax.rem(me_y - step + ny, ny)).wait_recv()
+
             down(layer, g, i, at)
             settle(at, end, hop)
 
-        @pl.when(active & (i == chunks - 1))
-        def _():
-            core_sum(layer, g)
+            @pl.when(i == chunks - 1)
+            def _():
+                core_sum(layer, g)
 
         return 0
 
@@ -477,7 +567,14 @@
     dma = pltpu.SemaphoreType.DMA
     ys = max(ny - 1, 1)
     half, chips = rows // CORES, n_cb // CORES
+    taps = gt.shape[1]
     scratch = [
+        pltpu.VMEM((groups, rows, d), tokens.dtype),
+        pltpu.VMEM(gain.shape, F32),
+        pltpu.VMEM((taps, layers, ff), F32),
+        pltpu.VMEM((taps, layers, ff), F32),
+        pltpu.VMEM(gb.shape, F32),
+        pltpu.VMEM(ub.shape, F32),
         pltpu.VMEM((layers, d, ff), BF16),
         pltpu.VMEM((layers, d, ff), BF16),
         pltpu.VMEM((layers, ff, d), BF16),
@@ -486,7 +583,10 @@
         pltpu.VMEM((groups, rows, LANES), F32),
         pltpu.VMEM((groups, rows, d), F32),
         pltpu.VMEM((layers, groups, 1, rows), F32),
-        pltpu.VMEM((layers, groups, n_ra - 1, 1, rows), F32),
+        pltpu.VMEM((layers, groups, ys, 1, rows), F32),
+        pltpu.VMEM((layers, groups, 1, rows), F32),
+        pltpu.VMEM((layers, groups, 2, 1, rows), F32),
+        pltpu.VMEM((layers, groups, 2, 1, rows), F32),
         pltpu.VMEM((n, ny, length, 2 * LANES), BF16),
         pltpu.VMEM((n, ys, length, 2 * LANES), BF16),
         pltpu.VMEM((n, ny, length, 2 * LANES), BF16),
@@ -495,8 +595,10 @@
         pltpu.VMEM((layers, groups, half, d), BF16),
         pltpu.VMEM((layers, groups, chips, half, d), BF16),
         pltpu.VMEM((layers, groups, CORES, half, d), BF16),
+        dma((6,)),
         dma((layers, chunks, 3)),
-        dma((layers, groups, n_ra - 1)), dma((layers, groups, n_ra - 1)),
+        dma((layers, groups, ys)), dma((layers, groups, ys)),
+        dma((layers, groups, 2)), dma((layers, groups, 2)),
         dma((n, ys)), dma((n, ys)),
         dma((n,)), dma((n,)),
         dma((n,)), dma((n,)),
@@ -512,7 +614,7 @@
     out = pl.pallas_call(
         functools.partial(kernel, dims),
         out_shape=jax.ShapeDtypeStruct((groups, rows, d), tokens.dtype),
-        in_specs=[vmem, vmem, hbm, hbm, vmem, vmem, vmem, vmem, hbm],
+        in_specs=[hbm] * 9,
         out_specs=vmem,
         scratch_shapes=scratch,
         compiler_params=pltpu.CompilerParams(

time: 191 us -> 187 us (0.979)
  Pallas kernels: 189 us -> 185 us
    pallas_call x1, Pallas kernels: 189 us -> 185 us  [per_device(): pl.pallas_call(functools.partial(kernel, dims), out_shape=jax.ShapeDtypeS...]
where the time goes in v3:
time: 187 us; the launch traced here: 186 us
  Pallas kernels  185 us (99%)
  local copies, waits for them, and re-layouts  1.87 us (1%)
    pallas_call x1, Pallas kernels, per_device(): pl.pallas_call(functools.partial(kernel, dims), out_shape=jax.ShapeDtypeS...  185 us

profile of v3, /device:TPU:0, one launch (start us, length us, event | category | flops | bytes accessed | tf_op | source)
XLA Modules:
  0.0 186.5 jit_solution(6023925651939875816)
XLA Ops:
  0.0 184.6 %blocks.1 = bf16[4,128,512]{2,1,0:T(8,128)(2,1)} custom-call(bf16[4,128,512]{2,1,0:T(8,128)(2,1)} %tok_hbm.1, f32[2,512]{1,0:T(2,128)} %gain_hbm.1, bf16[2,512,2816]{2,1,0:T(8,128)(2,1)} %gw_hbm.1, bf16[2,512,2816]{2,1,0:T(8,128)(2,1)} %uw_hbm.1, f32[3,2,2816]{2,1,0:T(2,128)} %bitcast.2, f32[3,2,2816]{2,1,0:T(2,128)} %bitcast.3, f32[2,2816]{1,0:T(2,128)} %gb_hbm.1, ...), custom_call_target="tpu_custom_call" | custom-call | tf_op jit(solution)/shard_map/blocks/pallas_call | solution.py:614
  184.6 1.9 %copy.11 = bf16[4,128,512]{2,1,0:T(8,128)(2,1)} copy(bf16[4,128,512]{2,1,0:T(8,128)(2,1)} %blocks.1) | data formatting | bytes 1048576

commit v4 on v3

--- a/solution.py
+++ b/solution.py
@@ -22,11 +22,11 @@
 def kernel(
     dims,
     tok_hbm, gain_hbm, gw_hbm, uw_hbm, gt_hbm, ut_hbm, gb_hbm, ub_hbm, dw_hbm,
-    out_ref,
-    tok_ref, gain_ref, gt_ref, ut_ref, gb_ref, ub_ref,
+    out_hbm,
+    out_ref, tok_ref, gain_ref, gt_ref, ut_ref, gb_ref, ub_ref,
     gw_ref, uw_ref, dw_ref, carried, scaled, inv, acc,
     sq_own, sq_y, sq_sum, sq_fwd, sq_z, part, y_in, z_in, hid, c_out, c_in, c_sum, c_all,
-    i_sem, w_sem, sq_s, sq_r, sz_s, sz_r, y_s, y_r, z_s, z_r, wz_s, wz_r, wy_s, wy_r, hy_s, hy_r, hz_s, hz_r, nz_s, nz_r, ny_s, ny_r, c_s, c_r, cs_s, cs_r, ca_s, ca_r,
+    o_sem, i_sem, w_sem, sq_s, sq_r, sz_s, sz_r, y_s, y_r, z_s, z_r, wz_s, wz_r, wy_s, wy_r, hy_s, hy_r, hz_s, hz_r, nz_s, nz_r, ny_s, ny_r, c_s, c_r, cs_s, cs_r, ca_s, ca_r,
 ):
     n_ra, n_cb, nz, groups, rows, length, layers, width, chunks = dims
     ny = n_ra // nz
@@ -117,14 +117,14 @@
         to = lax.rem(me_y + step, ny)
         return remote(
             part.at[at, to, first], y_in.at[at, step - 1, first],
-            y_s.at[at, step - 1], y_r.at[at, step - 1], ra=me_z * ny + to,
+            y_s.at[step - 1], y_r.at[at, step - 1], ra=me_z * ny + to,
         )
 
     def late_copy(at, step):
         to = lax.rem(me_y + step, ny)
         return remote(
             part.at[at, to, rest], y_in.at[at, step - 1, rest],
-            wy_s.at[at, step - 1], wy_r.at[at, step - 1], ra=me_z * ny + to,
+            wy_s.at[step - 1], wy_r.at[at, step - 1], ra=me_z * ny + to,
         )
 
     def along(end):
@@ -132,20 +132,20 @@
 
     def z_copy(at, end):
         return remote(
-            part.at[at, me_y, first], z_in.at[at, 0, first], z_s.at[at], z_r.at[at],
+            part.at[at, me_y, first], z_in.at[at, 0, first], z_s.at[end], z_r.at[at],
             ra=along(end),
         )
 
     def wide_copy(at, end):
         return remote(
-            part.at[at, :, rest], z_in.at[at, :, rest], wz_s.at[at], wz_r.at[at], ra=along(end)
+            part.at[at, :, rest], z_in.at[at, :, rest], wz_s.at[end], wz_r.at[at], ra=along(end)
         )
 
     def hy_copy(at, step, y):
         to = lax.rem(me_y + step, ny)
         block = hid.at[at, y]
         return remote(
-            block, block, hy_s.at[at, step - 1], hy_r.at[at, step - 1], ra=me_z * ny + to
+            block, block, hy_s.at[step - 1], hy_r.at[at, step - 1], ra=me_z * ny + to
         )
 
     spread = int(length * SPREAD) // 16 * 16
@@ -153,16 +153,16 @@
 
     def hz_copy(at, end):
         rows_of = hid.at[at, :, both]
-        return remote(rows_of, rows_of, hz_s.at[at], hz_r.at[at], ra=along(1 - end))
+        return remote(rows_of, rows_of, hz_s.at[end], hz_r.at[at], ra=along(1 - end))
 
     def own_copy(at, end):
         rows_of = hid.at[at, me_y, own]
-        return remote(rows_of, rows_of, nz_s.at[at], nz_r.at[at], ra=along(1 - end))
-
-    def cross_copy(at, step, y):
+        return remote(rows_of, rows_of, nz_s.at[end], nz_r.at[at], ra=along(1 - end))
+
+    def cross_copy(at, end, step, y):
         rows_of = hid.at[at, y, own]
         return remote(
-            rows_of, rows_of, ny_s.at[at, step - 1], ny_r.at[at, step - 1],
+            rows_of, rows_of, ny_s.at[end, step - 1], ny_r.at[at, step - 1],
             ra=me_z * ny + lax.rem(me_y + step, ny),
         )
 
@@ -307,30 +307,32 @@
         )
         acc[g] += jnp.dot(hidden, dw_ref[layer, depth, :], preferred_element_type=F32)
 
-    def settle(at, end, hop):
-        for step in range(1, ny):
-            y_copy(at, step).wait_send()
-
-        @pl.when(hop < nz - 1)
-        def _():
-            z_copy(at, end).wait_send()
-            wide_copy(at, end).wait_send()
-
-        @pl.when(hop == nz - 1)
-        def _():
-            for step in range(1, ny):
-                late_copy(at, step).wait_send()
-                hy_copy(at, step, me_y).wait_send()
-
-        @pl.when(hop > 0)
-        def _():
-            hz_copy(at, end).wait_send()
-            own_copy(at, end).wait_send()
-
-        @pl.when(hop < nz - 1)
-        def _():
-            for step in range(1, ny):
-                cross_copy(at, step, me_y).wait_send()
+    def sent(ref, semaphore):
+        remote(ref, ref, semaphore, semaphore, cb=me_cb + 1 - 2 * core).wait_send()
+
+    def settle():
+        for step in range(1, ny):
+            sent(y_in.at[:, step - 1, first], y_s.at[step - 1])
+        for end in range(2):
+            many = pl.ds(0, layers * ((per_layer + 1 - end) // 2))
+
+            @pl.when(me_z == end * (nz - 1))
+            def _():
+                for step in range(1, ny):
+                    sent(y_in.at[many, step - 1, rest], wy_s.at[step - 1])
+                    sent(hid.at[many, 0], hy_s.at[step - 1])
+
+            @pl.when(me_z != end * (nz - 1))
+            def _():
+                sent(z_in.at[many, 0, first], z_s.at[end])
+                sent(z_in.at[many, :, rest], wz_s.at[end])
+                for step in range(1, ny):
+                    sent(hid.at[many, 0, own], ny_s.at[end, step - 1])
+
+            @pl.when(me_z != (1 - end) * (nz - 1))
+            def _():
+                sent(hid.at[many, :, both], hz_s.at[end])
+                sent(hid.at[many, 0, own], nz_s.at[end])
 
     def half_of(which):
         return pl.ds(pl.multiple_of(which * half_rows, half_rows), half_rows)
@@ -356,6 +358,9 @@
         c_all[layer, g, core] = value.astype(BF16)
         all_copy(layer, g, core).start()
 
+    def out_copy(g):
+        return pltpu.make_async_copy(out_ref.at[g], out_hbm.at[g], o_sem.at[g])
+
     def finish(layer, g):
         all_copy(layer, g, 1 - core).wait_recv()
         all_copy(layer, g, core).wait_send()
@@ -371,6 +376,7 @@
         @pl.when(layer == layers - 1)
         def _():
             out_ref[g] = carried[g].astype(out_ref.dtype)
+            out_copy(g).start()
 
     def enter(g):
         carried[g] = tok_ref[g].astype(F32)
@@ -442,7 +448,7 @@
                 if far < nz - 1:
                     own_copy(at, end).start()
                 for step in range(1, ny):
-                    cross_copy(at, step, me_y).start()
+                    cross_copy(at, end, step, me_y).start()
 
         for far in range(nz - 2, 0, -1):
             active, at, end, hop, layer = place(gather_lag + LAG_HZ * far)
@@ -536,10 +542,9 @@
             @pl.when(hop < nz - 1)
             def _():
                 for step in range(1, ny):
-                    cross_copy(at, step, lax.rem(me_y - step + ny, ny)).wait_recv()
+                    cross_copy(at, end, step, lax.rem(me_y - step + ny, ny)).wait_recv()
 
             down(layer, g, i, at)
-            settle(at, end, hop)
 
             @pl.when(i == chunks - 1)
             def _():
@@ -548,6 +553,9 @@
         return 0
 
     lax.fori_loop(0, stride * (layers - 1) + per_layer + total_lag, body, 0)
+    settle()
+    for g in range(groups):
+        out_copy(g).wait()
 
 
 def per_device(n_ra, n_cb, tokens, gain, gw, uw, gt, ut, gb, ub, dw):
@@ -562,13 +570,13 @@
     chunks = ff // width
     n = layers * groups * chunks
     dims = (n_ra, n_cb, nz, groups, rows, length, layers, width, chunks)
-    vmem = pl.BlockSpec(memory_space=pltpu.VMEM)
     hbm = pl.BlockSpec(memory_space=pl.ANY)
     dma = pltpu.SemaphoreType.DMA
     ys = max(ny - 1, 1)
     half, chips = rows // CORES, n_cb // CORES
     taps = gt.shape[1]
     scratch = [
+        pltpu.VMEM((groups, rows, d), tokens.dtype),
         pltpu.VMEM((groups, rows, d), tokens.dtype),
         pltpu.VMEM(gain.shape, F32),
         pltpu.VMEM((taps, layers, ff), F32),
@@ -595,18 +603,18 @@
         pltpu.VMEM((layers, groups, half, d), BF16),
         pltpu.VMEM((layers, groups, chips, half, d), BF16),
         pltpu.VMEM((layers, groups, CORES, half, d), BF16),
-        dma((6,)),
+        dma((groups,)), dma((6,)),
         dma((layers, chunks, 3)),
         dma((layers, groups, ys)), dma((layers, groups, ys)),
         dma((layers, groups, 2)), dma((layers, groups, 2)),
-        dma((n, ys)), dma((n, ys)),
-        dma((n,)), dma((n,)),
-        dma((n,)), dma((n,)),
-        dma((n, ys)), dma((n, ys)),
-        dma((n, ys)), dma((n, ys)),
-        dma((n,)), dma((n,)),
-        dma((n,)), dma((n,)),
-        dma((n, ys)), dma((n, ys)),
+        dma((ys,)), dma((n, ys)),
+        dma((2,)), dma((n,)),
+        dma((2,)), dma((n,)),
+        dma((ys,)), dma((n, ys)),
+        dma((ys,)), dma((n, ys)),
+        dma((2,)), dma((n,)),
+        dma((2,)), dma((n,)),
+        dma((2, ys)), dma((n, ys)),
         dma((layers, groups)), dma((layers, groups)),
         dma((layers, groups, max(chips - 1, 1))), dma((layers, groups, max(chips - 1, 1))),
         dma((layers, groups)), dma((layers, groups)),
@@ -615,7 +623,7 @@
         functools.partial(kernel, dims),
         out_shape=jax.ShapeDtypeStruct((groups, rows, d), tokens.dtype),
         in_specs=[hbm] * 9,
-        out_specs=vmem,
+        out_specs=hbm,
         scratch_shapes=scratch,
         compiler_params=pltpu.CompilerParams(
             collective_id=0, has_side_effects=True, vmem_limit_bytes=60 * 1024 * 1024

time: 187 us -> 180 us (0.963)
  Pallas kernels: 185 us -> 178 us
    pallas_call x1, Pallas kernels: 185 us -> 178 us  [per_device(): pl.pallas_call(functools.partial(kernel, dims), out_shape=jax.ShapeDtypeS...]
where the time goes in v4:
time: 180 us
  Pallas kernels  178 us (99%)
  local copies, waits for them, and re-layouts  1.87 us (1%)
    pallas_call x1, Pallas kernels, per_device(): pl.pallas_call(functools.partial(kernel, dims), out_shape=jax.ShapeDtypeS...  178 us

profile of v4, /device:TPU:0, one launch (start us, length us, event | category | flops | bytes accessed | tf_op | source)
XLA Modules:
  0.0 180.0 jit_solution(5377826828895506432)
XLA Ops:
  0.0 178.1 %blocks.1 = bf16[4,128,512]{2,1,0:T(8,128)(2,1)} custom-call(bf16[4,128,512]{2,1,0:T(8,128)(2,1)} %tok_hbm.1, f32[2,512]{1,0:T(2,128)} %gain_hbm.1, bf16[2,512,2816]{2,1,0:T(8,128)(2,1)} %gw_hbm.1, bf16[2,512,2816]{2,1,0:T(8,128)(2,1)} %uw_hbm.1, f32[3,2,2816]{2,1,0:T(2,128)} %bitcast.2, f32[3,2,2816]{2,1,0:T(2,128)} %bitcast.3, f32[2,2816]{1,0:T(2,128)} %gb_hbm.1, ...), custom_call_target="tpu_custom_call" | custom-call | tf_op jit(solution)/shard_map/blocks/pallas_call | solution.py:622
  178.1 1.9 %copy.11 = bf16[4,128,512]{2,1,0:T(8,128)(2,1)} copy(bf16[4,128,512]{2,1,0:T(8,128)(2,1)} %blocks.1) | data formatting | bytes 1048576

commit v5 on v4

--- a/solution.py
+++ b/solution.py
@@ -13,7 +13,7 @@
 CORES = 2
 LAG_Y, LAG_Z, LAG_HY, LAG_HZ = 4, 4, 4, 4
 TAIL_CHIP, TAIL_SUM, TAIL_END = 1, 4, 5
-SPLIT, SPREAD = 1 / 2, 1 / 2
+SPLIT, SPREAD = 5 / 8, 5 / 8
 
 MESH = pl.DeviceIdType.MESH
 F32, BF16 = jnp.float32, jnp.bfloat16

time: 180 us -> 179 us (level)
  no operation moved by 1% of the time
where the time goes in v5:
time: 179 us
  Pallas kernels  177 us (99%)
  local copies, waits for them, and re-layouts  1.87 us (1%)
    pallas_call x1, Pallas kernels, per_device(): pl.pallas_call(functools.partial(kernel, dims), out_shape=jax.ShapeDtypeS...  177 us

profile of v5, /device:TPU:0, one launch (start us, length us, event | category | flops | bytes accessed | tf_op | source)
XLA Modules:
  0.0 178.6 jit_solution(7443454897843257020)
XLA Ops:
  0.0 176.8 %blocks.1 = bf16[4,128,512]{2,1,0:T(8,128)(2,1)} custom-call(bf16[4,128,512]{2,1,0:T(8,128)(2,1)} %tok_hbm.1, f32[2,512]{1,0:T(2,128)} %gain_hbm.1, bf16[2,512,2816]{2,1,0:T(8,128)(2,1)} %gw_hbm.1, bf16[2,512,2816]{2,1,0:T(8,128)(2,1)} %uw_hbm.1, f32[3,2,2816]{2,1,0:T(2,128)} %bitcast.2, f32[3,2,2816]{2,1,0:T(2,128)} %bitcast.3, f32[2,2816]{1,0:T(2,128)} %gb_hbm.1, ...), custom_call_target="tpu_custom_call" | custom-call | tf_op jit(solution)/shard_map/blocks/pallas_call | solution.py:622
  176.8 1.9 %copy.11 = bf16[4,128,512]{2,1,0:T(8,128)(2,1)} copy(bf16[4,128,512]{2,1,0:T(8,128)(2,1)} %blocks.1) | data formatting | bytes 1048576
